TPU v7x, 32 devices: a whole 2x2x4 slice. The times are simulated.
32 devices in a mesh: fs: 8 (over z, y), tp: 4 (over x, core).
Axes of the slice: x: 2, y: 2, z: 4, core: 2. Of those that a mesh axis runs over, the one named last changes fastest.
Arguments:
- tokens: bfloat16 [640, 3072], P('tp'), may hold values from -6 to 6
- gain_first: float32 [3072], replicated, may hold values from 0.1 to 1.9
- gain_second: float32 [3072], replicated, may hold values from 0.1 to 1.9
- gate_first: float32 [3072, 8192], P('fs', 'tp'), may hold values from -0.109375 to 0.109375
- up_first: float32 [3072, 8192], P('fs', 'tp'), may hold values from -0.109375 to 0.109375
- down_first: float32 [8192, 3072], P('fs', 'tp'), may hold values from -0.09375 to 0.09375
- gate_second: float32 [3072, 8192], P('fs', 'tp'), may hold values from -0.109375 to 0.109375
- up_second: float32 [3072, 8192], P('fs', 'tp'), may hold values from -0.109375 to 0.109375
- down_second: float32 [8192, 3072], P('fs', 'tp'), may hold values from -0.09375 to 0.09375
Outputs:
- result_rows: bfloat16 [640, 3072], P('tp')
- serve_gate_first: bfloat16 [3072, 8192], P(None, 'fs')
- serve_up_first: bfloat16 [3072, 8192], P(None, 'fs')
- serve_down_first: bfloat16 [8192, 3072], P('fs')
- serve_gate_second: bfloat16 [3072, 8192], P(None, 'fs')
- serve_up_second: bfloat16 [3072, 8192], P(None, 'fs')
- serve_down_second: bfloat16 [8192, 3072], P('fs')
All inputs are finite; a program needn't handle non-finite values.
Results may differ from a plain program's by a relative error of at most 0.011.
Values may be sent and summed in bfloat16 or wider, within the bound.
A program may use at most 192 MiB of HBM per device.

v0:
```python
import jax
import jax.numpy as jnp
from jax import lax
from jax.sharding import PartitionSpec as P


def plain_norm(values):
    values = values.astype(jnp.float32)
    center = jnp.mean(values, axis=-1, keepdims=True)
    spread = jnp.mean(jnp.square(values - center), axis=-1, keepdims=True)
    return (values - center) * lax.rsqrt(spread + 1e-05)


def sum_over_hidden(partial_value):
    pieces = lax.all_to_all(
        partial_value.astype(jnp.bfloat16), "fs", split_axis=1, concat_axis=0, tiled=True
    )
    rows = partial_value.shape[0]
    pieces = pieces.reshape(-1, rows, pieces.shape[1]).astype(jnp.float32)
    summed = jnp.sum(pieces, axis=0).astype(jnp.bfloat16)
    return lax.all_gather(summed, "fs", axis=1, tiled=True).astype(jnp.float32)


def regroup(folded):
    spread = lax.all_to_all(folded, "tp", split_axis=0, concat_axis=1, tiled=True)
    parts = lax.axis_size("fs")
    rows = spread.shape[0]
    owned = lax.all_to_all(spread, "fs", split_axis=1, concat_axis=0, tiled=True)
    owned = owned.reshape(parts, rows, owned.shape[1])
    whole = lax.all_gather(owned, "tp", axis=1, tiled=True)
    return whole.reshape(-1, whole.shape[2])


def half_step(normed, scales, w_gate, w_rising, w_down):
    gate_part = jnp.dot(normed, w_gate, preferred_element_type=jnp.float32)
    rising = jnp.dot(normed, w_rising, preferred_element_type=jnp.float32)
    hidden = (jax.nn.silu(gate_part) * rising).astype(jnp.bfloat16)
    partial_value = jnp.dot(hidden, w_down, preferred_element_type=jnp.float32)
    block = sum_over_hidden(partial_value)
    mixed = 1.6817928 * scales[None, :] * normed.astype(jnp.float32) + 0.5 * block
    return plain_norm(mixed).astype(jnp.bfloat16)


def on_device(
    tokens,
    gain_first,
    gain_second,
    gate_first,
    up_first,
    down_first,
    gate_second,
    up_second,
    down_second,
):
    row_count = gate_first.shape[0]
    offset = lax.axis_index("fs") * row_count

    def fold_gain(weight, scales):
        picked = lax.dynamic_slice_in_dim(scales, offset, row_count, 0)
        return (picked[:, None] * weight).astype(jnp.bfloat16)

    serve_gate_first = regroup(fold_gain(gate_first, gain_first))
    serve_up_first = regroup(fold_gain(up_first, gain_first))
    serve_down_first = lax.all_gather(down_first.astype(jnp.bfloat16), "tp", axis=1, tiled=True)
    serve_gate_second = regroup(fold_gain(gate_second, gain_second))
    serve_up_second = regroup(fold_gain(up_second, gain_second))
    serve_down_second = lax.all_gather(down_second.astype(jnp.bfloat16), "tp", axis=1, tiled=True)
    normed_zero = plain_norm(tokens).astype(jnp.bfloat16)
    normed_one = half_step(
        normed_zero, gain_first, serve_gate_first, serve_up_first, serve_down_first
    )
    result_rows = half_step(
        normed_one, gain_second, serve_gate_second, serve_up_second, serve_down_second
    )
    return (
        result_rows,
        serve_gate_first,
        serve_up_first,
        serve_down_first,
        serve_gate_second,
        serve_up_second,
        serve_down_second,
    )


def solution(mesh):
    placed = (
        P("tp", None),
        P(),
        P(),
        P("fs", "tp"),
        P("fs", "tp"),
        P("fs", "tp"),
        P("fs", "tp"),
        P("fs", "tp"),
        P("fs", "tp"),
    )
    return jax.shard_map(
        on_device,
        mesh=mesh,
        in_specs=placed,
        out_specs=(
            P("tp", None),
            P(None, "fs"),
            P(None, "fs"),
            P("fs", None),
            P(None, "fs"),
            P(None, "fs"),
            P("fs", None),
        ),
        check_vma=False,
    )
```

profile of v0, /device:TPU:0, one launch (start us, length us, event | category | flops | bytes accessed | tf_op | source)
XLA Modules:
  0.0 523.0 jit_solution(2696292961990616382)
XLA Ops:
  8.0 3.7 multiply_convert_fusion.3
  11.7 24.1 %all_to_all.154 = bf16[4,96,2048]{2,1,0:T(8,128)(2,1)S(1)} all-to-all(bf16[4,96,2048]{2,1,0:T(8,128)(2,1)S(1)} %bitcast.44), channel_id=1, replica_groups=mesh['fs'=8,'tp'=4] {'tp'}, dimensions={0} | all-to-all | bytes 3145728 | tf_op jit(solution)/shard_map/all_to_all | solution.py:25
  41.2 42.3 %all_to_all.155 = bf16[96,8,1024]{2,0,1:T(8,128)(2,1)S(1)} all-to-all(bf16[96,8,1024]{2,0,1:T(8,128)(2,1)S(1)} %copy.29), channel_id=1, replica_groups=mesh['fs'=8,'tp'=4] {'fs'}, dimensions={1} | all-to-all | bytes 3145728 | tf_op jit(solution)/shard_map/all_to_all | solution.py:28
  85.6 36.1 %all_to_all.156 = bf16[4,96,2048]{2,1,0:T(8,128)(2,1)S(1)} all-to-all(bf16[4,96,2048]{2,1,0:T(8,128)(2,1)S(1)} %bitcast.42), channel_id=1, replica_groups=mesh['fs'=8,'tp'=4] {'tp'}, dimensions={0} | all-to-all | bytes 3145728 | tf_op jit(solution)/shard_map/all_to_all | solution.py:25
  124.2 39.1 %all_to_all.157 = bf16[96,8,1024]{2,0,1:T(8,128)(2,1)S(1)} all-to-all(bf16[96,8,1024]{2,0,1:T(8,128)(2,1)S(1)} %copy.33), channel_id=1, replica_groups=mesh['fs'=8,'tp'=4] {'fs'}, dimensions={1} | all-to-all | bytes 3145728 | tf_op jit(solution)/shard_map/all_to_all | solution.py:28
  166.8 3.9 multiply_convert_fusion.1
  170.7 39.8 %all_to_all.158 = bf16[4,96,2048]{2,1,0:T(8,128)(2,1)S(1)} all-to-all(bf16[4,96,2048]{2,1,0:T(8,128)(2,1)S(1)} %bitcast.45), channel_id=1, replica_groups=mesh['fs'=8,'tp'=4] {'tp'}, dimensions={0} | all-to-all | bytes 3145728 | tf_op jit(solution)/shard_map/all_to_all | solution.py:25
  215.8 51.1 %all_to_all.159 = bf16[96,8,1024]{2,0,1:T(8,128)(2,1)S(1)} all-to-all(bf16[96,8,1024]{2,0,1:T(8,128)(2,1)S(1)} %copy.38), channel_id=1, replica_groups=mesh['fs'=8,'tp'=4] {'fs'}, dimensions={1} | all-to-all | bytes 3145728 | tf_op jit(solution)/shard_map/all_to_all | solution.py:28
  269.0 26.1 %all_to_all.160 = bf16[4,96,2048]{2,1,0:T(8,128)(2,1)S(1)} all-to-all(bf16[4,96,2048]{2,1,0:T(8,128)(2,1)S(1)} %bitcast.43), channel_id=1, replica_groups=mesh['fs'=8,'tp'=4] {'tp'}, dimensions={0} | all-to-all | bytes 3145728 | tf_op jit(solution)/shard_map/all_to_all | solution.py:25
  297.6 39.2 %all_to_all.161 = bf16[96,8,1024]{2,0,1:T(8,128)(2,1)S(1)} all-to-all(bf16[96,8,1024]{2,0,1:T(8,128)(2,1)S(1)} %copy.42), channel_id=1, replica_groups=mesh['fs'=8,'tp'=4] {'fs'}, dimensions={1} | all-to-all | bytes 3145728 | tf_op jit(solution)/shard_map/all_to_all | solution.py:28
  342.0 9.7 %copy.31 = bf16[8,384,1024]{2,1,0:T(8,128)(2,1)} copy(bf16[8,384,1024]{2,0,1:T(8,128)(2,1)} %all-gather.7.cloned.1.call-done) | data formatting | bytes 12582912 | tf_op jit(solution)/shard_map/all_gather | solution.py:30
  351.7 9.2 %copy.35 = bf16[8,384,1024]{2,1,0:T(8,128)(2,1)} copy(bf16[8,384,1024]{2,0,1:T(8,128)(2,1)} %all-gather.9.cloned.1.call-done) | data formatting | bytes 12582912 | tf_op jit(solution)/shard_map/all_gather | solution.py:30
  362.3 7.0 %convolution_convert_fusion.1 = bf16[160,3072]{1,0:T(8,128)(2,1)S(1)} fusion(bf16[1024,3072]{1,0:T(8,128)(2,1)} %all-gather.11.cloned.1.call-done, bf16[3072,1024]{1,0:T(8,128)(2,1)} %bitcast.38, f32[160,1024]{1,0:T(8,128)S(1)} %fusion.14, bf16[160,3072]{1,0:T(8,128)(2,1)S(1)} %copy-done.1, f32[160]{0:T(256)S(1)} %add_rsqrt_fusion.2, ...), kind=kOutput, calls=%fused_computation.1 | convolution fusion | flops 2016706560 | bytes 15205632 | tf_op jit(solution)/shard_map/dot_general | solution.py:38
  370.3 3.8 all-to-all-start.4
  374.1 9.1 %copy.40 = bf16[8,384,1024]{2,1,0:T(8,128)(2,1)} copy(bf16[8,384,1024]{2,0,1:T(8,128)(2,1)} %all-gather.13.cloned.1.call-done) | data formatting | bytes 12582912 | tf_op jit(solution)/shard_map/all_gather | solution.py:30
  383.7 9.0 %copy.44 = bf16[8,384,1024]{2,1,0:T(8,128)(2,1)} copy(bf16[8,384,1024]{2,0,1:T(8,128)(2,1)} %all-gather.15.cloned.1.call-done) | data formatting | bytes 12582912 | tf_op jit(solution)/shard_map/all_gather | solution.py:30
  392.7 5.5 %all-to-all-done.4 = bf16[160,8,384]{2,0,1:T(8,128)(2,1)S(1)} async-done(((bf16[160,8,384]{2,0,1:T(8,128)(2,1)}), bf16[160,8,384]{2,0,1:T(8,128)(2,1)S(1)}, u32[]{:S(2)}, u32[]{:S(2)}) %all-to-all-start.4) | async-done | bytes 983072 | tf_op jit(solution)/shard_map/all_to_all | solution.py:15
  398.3 33.7 %all_gather.27 = bf16[160,3072]{1,0:T(8,128)(2,1)S(1)} all-gather(bf16[160,384]{1,0:T(8,128)(2,1)S(1)} %reduce_sum.80), channel_id=1, replica_groups=mesh['fs'=8,'tp'=4] {'fs'}, dimensions={1}, use_global_device_ids=true | all-gather | bytes 1105920 | tf_op jit(solution)/shard_map/all_gather | solution.py:21
  436.0 6.9 %convolution_convert_fusion = bf16[160,3072]{1,0:T(8,128)(2,1)S(1)} fusion(bf16[1024,3072]{1,0:T(8,128)(2,1)} %all-gather.17.cloned.1.call-done, bf16[160,3072]{1,0:T(8,128)(2,1)S(1)} %multiply_convert_fusion.5, bf16[3072,1024]{1,0:T(8,128)(2,1)} %bitcast.40, f32[160,1024]{1,0:T(8,128)S(1)} %fusion.16), kind=kOutput, calls=%fused_computation | convolution fusion | flops 2014740480 | bytes 15204352 | tf_op jit(solution)/shard_map/dot_general | solution.py:38
  444.0 3.6 all-to-all-start.9
  447.6 23.0 %all-to-all-done.9 = bf16[160,8,384]{2,0,1:T(8,128)(2,1)S(1)} async-done(((bf16[160,8,384]{2,0,1:T(8,128)(2,1)}), bf16[160,8,384]{2,0,1:T(8,128)(2,1)S(1)}, u32[]{:S(2)}, u32[]{:S(2)}) %all-to-all-start.9) | async-done | bytes 983072 | tf_op jit(solution)/shard_map/all_to_all | solution.py:15
  470.6 33.6 %all_gather.31 = bf16[160,3072]{1,0:T(8,128)(2,1)S(1)} all-gather(bf16[160,384]{1,0:T(8,128)(2,1)S(1)} %reduce_sum.83), channel_id=1, replica_groups=mesh['fs'=8,'tp'=4] {'fs'}, dimensions={1}, use_global_device_ids=true | all-gather | bytes 1105920 | tf_op jit(solution)/shard_map/all_gather | solution.py:21
  506.9 6.1 %copy.54 = bf16[1024,3072]{1,0:T(8,128)(2,1)} copy(bf16[1024,3072]{1,0:T(8,128)(2,1)} %all-gather.11.cloned.1.call-done) | data formatting | bytes 12582912
  513.0 2.7 copy.55
  (79 shorter events, 40.1 us)
Async XLA Ops:
  7.2 334.9 %all-gather.7.cloned.1.call-start = ((), (), s32[]{:S(2)}) async-start(), calls=%async_computation.10 | async-start | bytes 7864320 | tf_op jit(solution)/shard_map/all_gather | solution.py:30
  85.5 266.2 %all-gather.9.cloned.1.call-start = ((), (), s32[]{:S(2)}) async-start(), calls=%async_computation.11 | async-start | bytes 7864320 | tf_op jit(solution)/shard_map/all_gather | solution.py:30
  163.3 2.1 copy-start.3
  165.3 1.4 copy-start.6
  165.3 196.9 %all-gather.11.cloned.1.call-start = ((), (), s32[]{:S(2)}) async-start(), calls=%async_computation.12 | async-start | bytes 7864320 | tf_op jit(solution)/shard_map/all_gather | solution.py:64
  166.7 207.4 %all-gather.13.cloned.1.call-start = ((), (), s32[]{:S(2)}) async-start(), calls=%async_computation.13 | async-start | bytes 7864320 | tf_op jit(solution)/shard_map/all_gather | solution.py:30
  269.0 114.7 %all-gather.15.cloned.1.call-start = ((), (), s32[]{:S(2)}) async-start(), calls=%async_computation.14 | async-start | bytes 7864320 | tf_op jit(solution)/shard_map/all_gather | solution.py:30
  336.8 2.1 copy-start.4
  338.8 97.2 %all-gather.17.cloned.1.call-start = ((), (), s32[]{:S(2)}) async-start(), calls=%async_computation.15 | async-start | bytes 7864320 | tf_op jit(solution)/shard_map/all_gather | solution.py:67
  340.2 1.2 copy-start.1
  351.7 9.2 %copy-start.2 = (bf16[8,384,1024]{2,1,0:T(8,128)(2,1)S(1)}, bf16[8,384,1024]{2,1,0:T(8,128)(2,1)}, u32[]{:S(2)}) copy-start(bf16[8,384,1024]{2,1,0:T(8,128)(2,1)} %copy.31) | copy-start | bytes 18874372
  369.3 4.8 copy-start.5
  370.3 27.8 %all-to-all-start.4 = ((bf16[160,8,384]{2,0,1:T(8,128)(2,1)}), bf16[160,8,384]{2,0,1:T(8,128)(2,1)S(1)}, u32[]{:S(2)}, u32[]{:S(2)}) async-start(bf16[160,8,384]{2,0,1:T(8,128)(2,1)} %bitcast.31), calls=%async_computation.4 | async-start | bytes 1966080 | tf_op jit(solution)/shard_map/all_to_all | solution.py:15
  432.0 2.8 copy-start
  444.0 26.5 %all-to-all-start.9 = ((bf16[160,8,384]{2,0,1:T(8,128)(2,1)}), bf16[160,8,384]{2,0,1:T(8,128)(2,1)S(1)}, u32[]{:S(2)}, u32[]{:S(2)}) async-start(bf16[160,8,384]{2,0,1:T(8,128)(2,1)} %bitcast.30), calls=%async_computation.9 | async-start | bytes 1966080 | tf_op jit(solution)/shard_map/all_to_all | solution.py:15
  505.4 7.6 %slice-start = ((s8[6291456]{0:T(1024)(128)(4,1)}), s8[4194304]{0:T(1024)(128)(4,1)S(1)}, s32[]{:S(2)}) async-start(s8[6291456]{0:T(1024)(128)(4,1)} %bitcast.34), calls=%async_computation.16 | async-start | bytes 8388608
  506.9 6.1 %slice-start.1 = ((s8[6291456]{0:T(1024)(128)(4,1)}), s8[2097152]{0:T(1024)(128)(4,1)S(1)}, s32[]{:S(2)}) async-start(s8[6291456]{0:T(1024)(128)(4,1)} %bitcast.34), calls=%async_computation.17 | async-start | bytes 4194304
Sparse Core Ops, SparseCore 0:
  85.6 57.7 all-gather.6
  165.4 61.2 all-gather.8
  228.8 46.1 all-gather.10
  276.5 50.4 all-gather.12
  338.9 44.6 all-gather.14
  385.7 46.3 all-gather.16
where the time goes:
time: 532 us; the launch traced here: 523 us
  blocking collectives  365 us (69%)
  local copies, waits for them, and re-layouts  74 us (14%)
  waiting for transfers between devices  29.1 us (5%)
  matrix products  16.4 us (3%)
  other arithmetic  16.1 us (3%)
  between operations  14.8 us (3%)
  starting transfers between devices  7.57 us (1%)
    all_to_all x4, blocking collectives, regroup(): lax.all_to_all(spread, 'fs', split_axis=1, concat_axis=0, tiled=True)  172 us
    all_to_all x4, blocking collectives, regroup(): lax.all_to_all(folded, 'tp', split_axis=0, concat_axis=1, tiled=True)  126 us
    all_gather x2, blocking collectives, sum_over_hidden(): return lax.all_gather(summed, 'fs', axis=1, tiled=True).astype(jnp.float32)  67.3 us
    all_gather x4, local copies, waits for them, and re-layouts, regroup(): whole = lax.all_gather(owned, 'tp', axis=1, tiled=True)  36.9 us
    all_to_all x2, waiting for transfers between devices, sum_over_hidden(): lax.all_to_all(partial_value.astype(jnp.bfloat16), 'fs', split_axis=1, co...  28.4 us
    all_to_all x12, local copies, waits for them, and re-layouts, regroup(): lax.all_to_all(spread, 'fs', split_axis=1, concat_axis=0, tiled=True)  18.8 us
    dot_general x2, matrix products, half_step(): partial_value = jnp.dot(hidden, w_down, preferred_element_type=jnp.float32)  13.9 us
  transfers between devices with their start and end apart: 8, of which 3 were waited for; matrix products, arithmetic and copies ran while one was open for 14% of the time, Pallas kernels for 0%

commit v1 on v0

--- a/solution.py
+++ b/solution.py
@@ -25,7 +25,9 @@
     spread = lax.all_to_all(folded, "tp", split_axis=0, concat_axis=1, tiled=True)
     parts = lax.axis_size("fs")
     rows = spread.shape[0]
-    owned = lax.all_to_all(spread, "fs", split_axis=1, concat_axis=0, tiled=True)
+    cells = jnp.split(spread, lax.axis_size("fs"), axis=1)
+    arrived = lax.all_to_all(jnp.stack(cells), "fs", 0, 0)
+    owned = jnp.concatenate(arrived, axis=0)
     owned = owned.reshape(parts, rows, owned.shape[1])
     whole = lax.all_gather(owned, "tp", axis=1, tiled=True)
     return whole.reshape(-1, whole.shape[2])

time: 532 us -> 508 us (0.955); the launches traced: 523 us -> 507 us
  local copies, waits for them, and re-layouts: 74 us -> 32.2 us
  waiting for transfers between devices: 29.1 us -> 49.1 us
  matrix products: 16.4 us -> 22 us
    all_gather x4 -> x0, local copies, waits for them, and re-layouts: 36.9 us -> none  [regroup(): whole = lax.all_gather(owned, 'tp', axis=1, tiled=True)]
    all_to_all x2, waiting for transfers between devices: 28.4 us -> 48.9 us  [sum_over_hidden(): lax.all_to_all(partial_value.astype(jnp.bfloat16), 'fs', split_axis=1, co...]
    all_to_all x12 -> x0, local copies, waits for them, and re-layouts: 18.8 us -> none  [regroup(): lax.all_to_all(spread, 'fs', split_axis=1, concat_axis=0, tiled=True)]
    unnamed x20 -> x60, local copies, waits for them, and re-layouts: 10.4 us -> 28.6 us
    all_to_all x4, blocking collectives: 172 us -> 165 us  [regroup(): arrived = lax.all_to_all(jnp.stack(cells), 'fs', 0, 0)]
    dot_general x2, matrix products: 2.55 us -> 8.05 us  [half_step(): gate_part = jnp.dot(normed, w_gate, preferred_element_type=jnp.float32)]
  transfers between devices with their start and end apart: 8 -> 8, of which waited for: 3 -> 2; matrix products, arithmetic and copies ran while one was open for 14% -> 6% of each run, Pallas kernels for 0% -> 0%
where the time goes in v1:
time: 508 us; the launch traced here: 507 us
  blocking collectives  361 us (71%)
  waiting for transfers between devices  49.1 us (10%)
  local copies, waits for them, and re-layouts  32.2 us (6%)
  matrix products  22 us (4%)
  other arithmetic  19.7 us (4%)
  between operations  14.6 us (3%)
  starting transfers between devices  8.66 us (2%)
    all_to_all x4, blocking collectives, regroup(): arrived = lax.all_to_all(jnp.stack(cells), 'fs', 0, 0)  165 us
    all_to_all x4, blocking collectives, regroup(): lax.all_to_all(folded, 'tp', split_axis=0, concat_axis=1, tiled=True)  130 us
    all_gather x2, blocking collectives, sum_over_hidden(): return lax.all_gather(summed, 'fs', axis=1, tiled=True).astype(jnp.float32)  66.2 us
    all_to_all x2, waiting for transfers between devices, sum_over_hidden(): lax.all_to_all(partial_value.astype(jnp.bfloat16), 'fs', split_axis=1, co...  48.9 us
    unnamed x60, local copies, waits for them, and re-layouts  28.6 us
    dot_general x2, matrix products, half_step(): partial_value = jnp.dot(hidden, w_down, preferred_element_type=jnp.float32)  14 us
  transfers between devices with their start and end apart: 8, of which 2 were waited for; matrix products, arithmetic and copies ran while one was open for 6% of the time, Pallas kernels for 0%

profile of v1, /device:TPU:0, one launch (start us, length us, event | category | flops | bytes accessed | tf_op | source)
XLA Modules:
  0.0 507.1 jit_solution(17659746832396600493)
XLA Ops:
  8.0 3.7 multiply_convert_fusion.3
  11.7 24.1 %all_to_all.122 = bf16[4,96,2048]{2,1,0:T(8,128)(2,1)S(1)} all-to-all(bf16[4,96,2048]{2,1,0:T(8,128)(2,1)S(1)} %bitcast.216), channel_id=1, replica_groups=mesh['fs'=8,'tp'=4] {'tp'}, dimensions={0} | all-to-all | bytes 3145728 | tf_op jit(solution)/shard_map/all_to_all | solution.py:25
  36.2 42.4 %all_to_all.123 = bf16[8,96,1024]{2,1,0:T(8,128)(2,1)} all-to-all(bf16[8,96,1024]{2,1,0:T(8,128)(2,1)S(1)} %fusion.34), channel_id=1, replica_groups=mesh['fs'=8,'tp'=4] {'fs'}, dimensions={0} | all-to-all | bytes 3145728 | tf_op jit(solution)/shard_map/all_to_all | solution.py:29
  81.9 39.3 %all_to_all.124 = bf16[4,96,2048]{2,1,0:T(8,128)(2,1)S(1)} all-to-all(bf16[4,96,2048]{2,1,0:T(8,128)(2,1)S(1)} %bitcast.182), channel_id=1, replica_groups=mesh['fs'=8,'tp'=4] {'tp'}, dimensions={0} | all-to-all | bytes 3145728 | tf_op jit(solution)/shard_map/all_to_all | solution.py:25
  121.6 39.8 %all_to_all.125 = bf16[8,96,1024]{2,1,0:T(8,128)(2,1)} all-to-all(bf16[8,96,1024]{2,1,0:T(8,128)(2,1)S(1)} %fusion.26), channel_id=1, replica_groups=mesh['fs'=8,'tp'=4] {'fs'}, dimensions={0} | all-to-all | bytes 3145728 | tf_op jit(solution)/shard_map/all_to_all | solution.py:29
  162.2 3.7 multiply_convert_fusion.1
  165.9 35.6 %all_to_all.126 = bf16[4,96,2048]{2,1,0:T(8,128)(2,1)S(1)} all-to-all(bf16[4,96,2048]{2,1,0:T(8,128)(2,1)S(1)} %bitcast.217), channel_id=1, replica_groups=mesh['fs'=8,'tp'=4] {'tp'}, dimensions={0} | all-to-all | bytes 3145728 | tf_op jit(solution)/shard_map/all_to_all | solution.py:25
  201.9 42.5 %all_to_all.127 = bf16[8,96,1024]{2,1,0:T(8,128)(2,1)} all-to-all(bf16[8,96,1024]{2,1,0:T(8,128)(2,1)S(1)} %fusion.18), channel_id=1, replica_groups=mesh['fs'=8,'tp'=4] {'fs'}, dimensions={0} | all-to-all | bytes 3145728 | tf_op jit(solution)/shard_map/all_to_all | solution.py:29
  244.5 3.3 convert_element_type.72
  247.8 31.0 %all_to_all.128 = bf16[4,96,2048]{2,1,0:T(8,128)(2,1)S(1)} all-to-all(bf16[4,96,2048]{2,1,0:T(8,128)(2,1)S(1)} %bitcast.183), channel_id=1, replica_groups=mesh['fs'=8,'tp'=4] {'tp'}, dimensions={0} | all-to-all | bytes 3145728 | tf_op jit(solution)/shard_map/all_to_all | solution.py:25
  279.1 39.8 %all_to_all.129 = bf16[8,96,1024]{2,1,0:T(8,128)(2,1)} all-to-all(bf16[8,96,1024]{2,1,0:T(8,128)(2,1)S(1)} %fusion.10), channel_id=1, replica_groups=mesh['fs'=8,'tp'=4] {'fs'}, dimensions={0} | all-to-all | bytes 3145728 | tf_op jit(solution)/shard_map/all_to_all | solution.py:29
  320.8 4.1 fusion.46
  324.9 7.1 %convolution_convert_fusion.1 = bf16[160,3072]{1,0:T(8,128)(2,1)S(1)} fusion(bf16[1024,3072]{1,0:T(8,128)(2,1)} %all-gather.11.cloned.1.call-done, bf16[3072,1024]{1,0:T(8,128)(2,1)} %bitcast.172, f32[160,1024]{1,0:T(8,128)S(1)} %fusion.46, bf16[160,3072]{1,0:T(8,128)(2,1)S(1)} %copy-done, f32[160]{0:T(256)S(1)} %add_rsqrt_fusion.2, ...), kind=kOutput, calls=%fused_computation.1 | convolution fusion | flops 2016706560 | bytes 15205632 | tf_op jit(solution)/shard_map/dot_general | solution.py:40
  333.1 3.6 all-to-all-start.4
  336.7 24.1 %all-to-all-done.4 = bf16[160,8,384]{2,0,1:T(8,128)(2,1)S(1)} async-done(((bf16[160,8,384]{2,0,1:T(8,128)(2,1)}), bf16[160,8,384]{2,0,1:T(8,128)(2,1)S(1)}, u32[]{:S(2)}, u32[]{:S(2)}) %all-to-all-start.4) | async-done | bytes 983072 | tf_op jit(solution)/shard_map/all_to_all | solution.py:15
  360.9 33.3 %all_gather.27 = bf16[160,3072]{1,0:T(8,128)(2,1)S(1)} all-gather(bf16[160,384]{1,0:T(8,128)(2,1)S(1)} %reduce_sum.80), channel_id=1, replica_groups=mesh['fs'=8,'tp'=4] {'fs'}, dimensions={1}, use_global_device_ids=true | all-gather | bytes 1105920 | tf_op jit(solution)/shard_map/all_gather | solution.py:21
  396.6 4.0 fusion.48
  400.6 6.9 %convolution_convert_fusion = bf16[160,3072]{1,0:T(8,128)(2,1)S(1)} fusion(bf16[1024,3072]{1,0:T(8,128)(2,1)} %all-gather.17.cloned.1.call-done, bf16[160,3072]{1,0:T(8,128)(2,1)S(1)} %multiply_convert_fusion.5, bf16[3072,1024]{1,0:T(8,128)(2,1)} %bitcast.178, f32[160,1024]{1,0:T(8,128)S(1)} %fusion.48), kind=kOutput, calls=%fused_computation | convolution fusion | flops 2014740480 | bytes 15204352 | tf_op jit(solution)/shard_map/dot_general | solution.py:40
  408.6 4.9 all-to-all-start.9
  413.4 24.8 %all-to-all-done.9 = bf16[160,8,384]{2,0,1:T(8,128)(2,1)S(1)} async-done(((bf16[160,8,384]{2,0,1:T(8,128)(2,1)}), bf16[160,8,384]{2,0,1:T(8,128)(2,1)S(1)}, u32[]{:S(2)}, u32[]{:S(2)}) %all-to-all-start.9) | async-done | bytes 983072 | tf_op jit(solution)/shard_map/all_to_all | solution.py:15
  438.3 33.0 %all_gather.31 = bf16[160,3072]{1,0:T(8,128)(2,1)S(1)} all-gather(bf16[160,384]{1,0:T(8,128)(2,1)S(1)} %reduce_sum.83), channel_id=1, replica_groups=mesh['fs'=8,'tp'=4] {'fs'}, dimensions={1}, use_global_device_ids=true | all-gather | bytes 1105920 | tf_op jit(solution)/shard_map/all_gather | solution.py:21
  473.9 6.4 %copy.70 = bf16[3072,1024]{1,0:T(8,128)(2,1)} copy(bf16[3072,1024]{1,0:T(8,128)(2,1)} %bitcast.169) | data formatting | bytes 12582912
  480.3 3.2 copy.71
  483.5 3.2 copy.72
  (111 shorter events, 28.9 us)
Async XLA Ops:
  7.2 313.6 %all-gather.7.cloned.1.call-start = ((), (), s32[]{:S(2)}) async-start(), calls=%async_computation.10 | async-start | bytes 7864320 | tf_op jit(solution)/shard_map/all_gather | solution.py:32
  78.6 246.3 %all-gather.11.cloned.1.call-start = ((), (), s32[]{:S(2)}) async-start(), calls=%async_computation.12 | async-start | bytes 7864320 | tf_op jit(solution)/shard_map/all_gather | solution.py:66
  81.9 243.0 %all-gather.9.cloned.1.call-start = ((), (), s32[]{:S(2)}) async-start(), calls=%async_computation.11 | async-start | bytes 7864320 | tf_op jit(solution)/shard_map/all_gather | solution.py:32
  161.4 0.7 copy-start.2
  161.4 235.2 %all-gather.13.cloned.1.call-start = ((), (), s32[]{:S(2)}) async-start(), calls=%async_computation.13 | async-start | bytes 7864320 | tf_op jit(solution)/shard_map/all_gather | solution.py:32
  244.4 156.2 %all-gather.17.cloned.1.call-start = ((), (), s32[]{:S(2)}) async-start(), calls=%async_computation.15 | async-start | bytes 7864320 | tf_op jit(solution)/shard_map/all_gather | solution.py:69
  247.8 152.8 %all-gather.15.cloned.1.call-start = ((), (), s32[]{:S(2)}) async-start(), calls=%async_computation.14 | async-start | bytes 7864320 | tf_op jit(solution)/shard_map/all_gather | solution.py:32
  318.9 1.2 copy-start
  332.0 4.6 copy-start.1
  333.1 27.7 %all-to-all-start.4 = ((bf16[160,8,384]{2,0,1:T(8,128)(2,1)}), bf16[160,8,384]{2,0,1:T(8,128)(2,1)S(1)}, u32[]{:S(2)}, u32[]{:S(2)}) async-start(bf16[160,8,384]{2,0,1:T(8,128)(2,1)} %bitcast.163), calls=%async_computation.4 | async-start | bytes 1966080 | tf_op jit(solution)/shard_map/all_to_all | solution.py:15
  408.6 29.6 %all-to-all-start.9 = ((bf16[160,8,384]{2,0,1:T(8,128)(2,1)}), bf16[160,8,384]{2,0,1:T(8,128)(2,1)S(1)}, u32[]{:S(2)}, u32[]{:S(2)}) async-start(bf16[160,8,384]{2,0,1:T(8,128)(2,1)} %bitcast.162), calls=%async_computation.9 | async-start | bytes 1966080 | tf_op jit(solution)/shard_map/all_to_all | solution.py:15
  472.4 7.9 %slice-start.4 = ((s8[6291456]{0:T(1024)(128)(4,1)}), s8[4194304]{0:T(1024)(128)(4,1)S(1)}, s32[]{:S(2)}) async-start(s8[6291456]{0:T(1024)(128)(4,1)} %bitcast.173), calls=%async_computation.20 | async-start | bytes 8388608
  473.9 6.4 %slice-start.5 = ((s8[6291456]{0:T(1024)(128)(4,1)}), s8[2097152]{0:T(1024)(128)(4,1)S(1)}, s32[]{:S(2)}) async-start(s8[6291456]{0:T(1024)(128)(4,1)} %bitcast.173), calls=%async_computation.21 | async-start | bytes 4194304
  473.9 9.6 %slice-start.2 = ((s8[6291456]{0:T(1024)(128)(4,1)}), s8[4194304]{0:T(1024)(128)(4,1)S(1)}, s32[]{:S(2)}) async-start(s8[6291456]{0:T(1024)(128)(4,1)} %bitcast.170), calls=%async_computation.18 | async-start | bytes 8388608
  480.3 3.2 slice-start.3
  480.3 7.2 %slice-start = ((s8[6291456]{0:T(1024)(128)(4,1)}), s8[4194304]{0:T(1024)(128)(4,1)S(1)}, s32[]{:S(2)}) async-start(s8[6291456]{0:T(1024)(128)(4,1)} %bitcast.165), calls=%async_computation.16 | async-start | bytes 8388608
  483.5 4.8 slice-start.1
  483.5 8.0 %slice-start.8 = ((s8[6291456]{0:T(1024)(128)(4,1)}), s8[2097152]{0:T(1024)(128)(4,1)S(1)}, s32[]{:S(2)}) async-start(s8[6291456]{0:T(1024)(128)(4,1)} %bitcast.179), calls=%async_computation.24 | async-start | bytes 4194304
  488.4 4.6 slice-start.9
  488.4 7.8 %slice-start.6 = ((s8[6291456]{0:T(1024)(128)(4,1)}), s8[2097152]{0:T(1024)(128)(4,1)S(1)}, s32[]{:S(2)}) async-start(s8[6291456]{0:T(1024)(128)(4,1)} %bitcast.176), calls=%async_computation.22 | async-start | bytes 4194304
  493.0 4.6 slice-start.7
Sparse Core Ops, SparseCore 0:
  78.7 61.0 all-gather.6
  142.0 57.5 all-gather.10
  201.1 48.5 all-gather.8
  251.2 54.4 all-gather.12
  307.7 44.3 all-gather.16
  353.6 46.3 all-gather.14
